TPU v7x, 32 devices: a whole 2x2x4 slice. The times are simulated.
32 devices in a mesh: grp: 2 (over x), fs: 4 (over z), tp: 4 (over y, core).
Axes of the slice: x: 2, y: 2, z: 4, core: 2. Of those that a mesh axis runs over, the one named last changes fastest.
Arguments:
- tokens: bfloat16 [960, 2048], P(('grp', 'tp')), parts along dimension 0, may hold values from -60 to 60
- route_expert: int32 [960, 4], P(('grp', 'tp')), parts along dimension 0, may hold values from 0 to 31, all different within a row; in each aligned block of 120 rows (0 to 119, 120 to 239, ...) at most 16 rows name the same one
- route_weight: float32 [960, 4], P(('grp', 'tp')), parts along dimension 0, may hold values from 0.05 to 1
- norm_gain: float32 [2048], P('tp'), may hold values from 0.1 to 1.9
- gate_train: float32 [32, 2048, 2048], P(None, 'tp', 'fs'), may hold values from -8 to 8
- up_train: float32 [32, 2048, 2048], P(None, 'tp', 'fs'), may hold values from -8 to 8
- down_train: float32 [32, 2048, 2048], P(None, 'tp', 'fs'), may hold values from -0.013671875 to 0.013671875
Outputs:
- gate_serve: bfloat16 [64, 2048, 2048], P(('grp', 'tp'), None, 'fs'), parts along dimension 0
- up_serve: bfloat16 [64, 2048, 2048], P(('grp', 'tp'), None, 'fs'), parts along dimension 0
- down_serve: bfloat16 [64, 2048, 2048], P(('grp', 'tp'), None, 'fs'), parts along dimension 0
- mixed: bfloat16 [960, 2048], P(('grp', 'tp'), 'fs'), parts along dimension 0
There are 2 independent parts, one for each index of `grp`. A program takes and returns all parts, laid end to end along the dimension named above; an argument that names none is the same for every part. Nothing has to cross between parts.
Inputs may be any that keep to these rules, and one draw needn't show every extreme that they name: `route_expert`: each row names 4 different experts; the rows of one device name each expert at most 16 times.
All inputs are finite; a program needn't handle non-finite values.
Results may differ from a plain program's by a relative error of at most 0.0087.
Values may be sent and summed in bfloat16 or wider, within the bound.
A program may use at most 320 MiB of HBM per device.

v0:
```python
import jax
import jax.numpy as jnp
from jax import lax
from jax.sharding import PartitionSpec as P

EXPERTS = 32
TOP = 4
CAP = 16


def activate(gate_pre, up_pre):
    clamped = jnp.minimum(gate_pre, 7.0)
    bounded = jnp.clip(up_pre, -7.0, 7.0)
    return (clamped * jax.nn.sigmoid(1.702 * clamped) * (bounded + 1.0)).astype(jnp.bfloat16)


def local(tokens, route_expert, route_weight, norm_gain, gate_train, up_train, down_train):
    gate_local = (gate_train * norm_gain[None, :, None]).astype(jnp.bfloat16)
    up_local = (up_train * norm_gain[None, :, None]).astype(jnp.bfloat16)
    down_local = down_train.astype(jnp.bfloat16)
    gate_serve, up_serve, down_serve = (
        lax.all_to_all(gate_local, "tp", split_axis=0, concat_axis=1, tiled=True),
        lax.all_to_all(up_local, "tp", split_axis=0, concat_axis=1, tiled=True),
        lax.all_to_all(down_local, "tp", split_axis=0, concat_axis=1, tiled=True),
    )
    tp_count = lax.axis_size("tp")
    fs_count = lax.axis_size("fs")
    per_dev = EXPERTS // tp_count
    tok_rows = tokens.shape[0]
    floated = tokens.astype(jnp.float32)
    normed = (
        floated * lax.rsqrt(jnp.mean(floated * floated, axis=-1, keepdims=True) + 1e-06)
    ).astype(jnp.bfloat16)
    flat_expert = route_expert.reshape(-1)
    expert_ids = jnp.arange(EXPERTS, dtype=jnp.int32)
    onehot = (flat_expert[:, None] == expert_ids[None, :]).astype(jnp.int32)
    slot_rank = jnp.sum((jnp.cumsum(onehot, axis=0) - 1) * onehot, axis=1)
    slot_index = flat_expert * CAP + slot_rank
    slot_hit = slot_index[:, None] == jnp.arange(EXPERTS * CAP, dtype=jnp.int32)[None, :]
    placement = slot_hit.reshape(tok_rows, TOP, EXPERTS * CAP).astype(jnp.float32)
    scatter_mat = jnp.sum(placement, axis=1).astype(jnp.bfloat16)
    combine_mat = jnp.sum(placement * route_weight[:, :, None], axis=1)
    col_width = normed.shape[1] // fs_count
    my_block = lax.axis_index("fs")
    column_part = lax.dynamic_slice_in_dim(normed, my_block * col_width, col_width, 1)
    buffer = lax.dot_general(
        scatter_mat, column_part, (((0,), (0,)), ((), ())), preferred_element_type=jnp.float32
    )
    arrived = lax.all_to_all(
        buffer.astype(jnp.bfloat16).reshape(EXPERTS, CAP, column_part.shape[1]),
        "tp",
        split_axis=0,
        concat_axis=0,
        tiled=True,
    )
    arrived = arrived.reshape(tp_count, per_dev, CAP, col_width)
    block_in = lax.all_gather(arrived, "fs", axis=3, tiled=True)
    gate_part = jnp.einsum(
        "secd,edf->secf", block_in, gate_serve, preferred_element_type=jnp.float32
    )
    up_part = jnp.einsum("secd,edf->secf", block_in, up_serve, preferred_element_type=jnp.float32)
    hidden = activate(gate_part, up_part)
    expert_out = jnp.einsum(
        "secf,efd->secd",
        lax.all_gather(hidden, "fs", axis=3, tiled=True),
        down_serve,
        preferred_element_type=jnp.float32,
    ).astype(jnp.bfloat16)
    outgoing = expert_out.reshape(tp_count * per_dev, CAP, down_serve.shape[2])
    returned_rows = lax.all_to_all(outgoing, "tp", split_axis=0, concat_axis=0, tiled=True).reshape(
        EXPERTS * CAP, down_serve.shape[2]
    )
    mixed = jnp.dot(
        combine_mat, returned_rows.astype(jnp.float32), precision=lax.Precision.HIGHEST
    ).astype(jnp.bfloat16)
    return (gate_serve, up_serve, down_serve, mixed)


def solution(mesh):
    return jax.shard_map(
        local,
        mesh=mesh,
        in_specs=(
            P(("grp", "tp"), None),
            P(("grp", "tp"), None),
            P(("grp", "tp"), None),
            P("tp"),
            P(None, "tp", "fs"),
            P(None, "tp", "fs"),
            P(None, "tp", "fs"),
        ),
        out_specs=(
            P(("grp", "tp"), None, "fs"),
            P(("grp", "tp"), None, "fs"),
            P(("grp", "tp"), None, "fs"),
            P(("grp", "tp"), "fs"),
        ),
        check_vma=False,
    )
```

profile of v0, /device:TPU:0, one launch (start us, length us, event | category | flops | bytes accessed | tf_op | source)
XLA Modules:
  0.0 668.9 jit_solution(10352614119127516276)
XLA Ops:
  7.2 1.1 convert_element_type.44
  8.3 1.2 multiply_reduce_fusion
  9.5 0.8 copy.41
  10.3 0.1 eq.36
  10.5 1.2 reduce-window.6
  11.6 0.2 slice_reduce_fusion
  11.9 0.1 bitcast_bitcast_fusion
  12.0 0.1 reduce_sum.39
  12.1 0.1 copy.44
  12.2 0.7 multiply_add_fusion
  12.9 0.9 convert_reduce_fusion
  13.9 1.2 convolution_convert_fusion
  15.0 4.3 all-to-all-start.3
  19.3 33.2 %multiply_convert_fusion = (bf16[32,512,512]{2,1,0:T(8,128)(2,1)}, bf16[32,512,512]{2,1,0:T(8,128)(2,1)}) fusion(f32[32,512,512]{2,1,0:T(8,128)} %param.12, f32[512]{0:T(512)} %param.10, f32[32,512,512]{2,1,0:T(8,128)} %param.11), kind=kLoop, calls=%fused_computation | loop fusion | flops 33554432 | bytes 100665344 | tf_op jit(solution)/shard_map/convert_element_type | solution.py:19
  52.5 194.1 %all_to_all.64 = bf16[32,512,512]{2,1,0:T(8,128)(2,1)} all-to-all(bf16[32,512,512]{2,1,0:T(8,128)(2,1)} %get-tuple-element.7), channel_id=1, replica_groups=mesh['grp'=2,'fs'=4,'tp'=4] {'tp'}, dimensions={0} | all-to-all | bytes 33554432 | tf_op jit(solution)/shard_map/all_to_all | solution.py:22
  246.6 7.1 %all-to-all-start.1 = ((bf16[32,512,512]{2,1,0:T(8,128)(2,1)}), bf16[32,512,512]{2,1,0:T(8,128)(2,1)}, u32[]{:S(2)}, u32[]{:S(2)}) async-start(bf16[32,512,512]{2,1,0:T(8,128)(2,1)} %get-tuple-element.6), calls=%async_computation.1 | async-start | bytes 33554432 | tf_op jit(solution)/shard_map/all_to_all | solution.py:23
  253.7 17.3 %convert_element_type.41 = bf16[32,512,512]{2,1,0:T(8,128)(2,1)} convert(f32[32,512,512]{2,1,0:T(8,128)} %param.13) | non-fusion elementwise | flops 8388608 | bytes 50331648 | tf_op jit(solution)/shard_map/convert_element_type | solution.py:20
  271.0 165.7 %all-to-all-done.1 = bf16[32,512,512]{2,1,0:T(8,128)(2,1)} async-done(((bf16[32,512,512]{2,1,0:T(8,128)(2,1)}), bf16[32,512,512]{2,1,0:T(8,128)(2,1)}, u32[]{:S(2)}, u32[]{:S(2)}) %all-to-all-start.1) | async-done | bytes 16777248 | tf_op jit(solution)/shard_map/all_to_all | solution.py:23
  436.7 7.0 %all-to-all-start.2 = ((bf16[32,512,512]{2,1,0:T(8,128)(2,1)}), bf16[32,512,512]{2,1,0:T(8,128)(2,1)}, u32[]{:S(2)}, u32[]{:S(2)}) async-start(bf16[32,512,512]{2,1,0:T(8,128)(2,1)} %convert_element_type.41), calls=%async_computation.2 | async-start | bytes 33554432 | tf_op jit(solution)/shard_map/all_to_all | solution.py:24
  443.6 0.0 all-gather.3.cloned.1.call-start
  443.7 0.8 copy.45
  444.6 0.0 all-gather.5.cloned.1.call-start
  444.6 13.8 %copy.38 = bf16[4,8,512,512]{3,2,0,1:T(8,128)(2,1)} copy(bf16[4,8,512,512]{3,2,1,0:T(8,128)(2,1)} %bitcast.59) | data formatting | bytes 33554432 | tf_op jit(solution)/shard_map/all_to_all | solution.py:22
  458.4 13.8 %copy.39 = bf16[4,8,512,512]{3,2,0,1:T(8,128)(2,1)} copy(bf16[4,8,512,512]{3,2,1,0:T(8,128)(2,1)} %bitcast.3) | data formatting | bytes 33554432 | tf_op jit(solution)/shard_map/all_to_all | solution.py:23
  472.3 22.4 %all-gather.3.cloned.1.call-done = bf16[4,8,16,2048]{3,2,0,1:T(8,128)(2,1)} async-done(((bf16[4,8,16,512]{3,2,0,1:T(8,128)(2,1)}), bf16[4,8,16,2048]{3,2,0,1:T(8,128)(2,1)}) %all-gather.3.cloned.1.call-update) | async-done | bytes 2097168 | tf_op jit(solution)/shard_map/all_gather | solution.py:57
  494.7 9.3 %fusion = f32[4,8,16,512]{3,2,0,1:T(8,128)S(1)} fusion(bf16[8,2048,512,1]{2,1,3,0:T(8,128)(2,1)} %bitcast.62, bf16[4,8,16,2048]{3,2,0,1:T(8,128)(2,1)} %all-gather.3.cloned.1.call-done), kind=kOutput, calls=%fused_computation.3 | convolution fusion | flops 1074003968 | bytes 19922944 | tf_op jit(solution)/shard_map/secd,edf->secf/dot_general | solution.py:58
  504.0 8.4 %fusion.4 = bf16[4,8,16,512]{3,2,0,1:T(8,128)(2,1)} fusion(bf16[8,2048,512,1]{2,1,3,0:T(8,128)(2,1)} %bitcast.64, bf16[4,8,16,2048]{3,2,0,1:T(8,128)(2,1)S(1)} %copy-done, f32[4,8,16,512]{3,2,0,1:T(8,128)S(1)} %fusion), kind=kOutput, calls=%fused_computation.10 | convolution fusion | flops 1076101120 | bytes 20447232 | tf_op jit(solution)/shard_map/secd,edf->secf/dot_general | solution.py:61
  512.4 114.3 %all-to-all-done.2 = bf16[32,512,512]{2,1,0:T(8,128)(2,1)} async-done(((bf16[32,512,512]{2,1,0:T(8,128)(2,1)}), bf16[32,512,512]{2,1,0:T(8,128)(2,1)}, u32[]{:S(2)}, u32[]{:S(2)}) %all-to-all-start.2) | async-done | bytes 16777248 | tf_op jit(solution)/shard_map/all_to_all | solution.py:24
  626.7 13.8 %copy.40 = bf16[4,8,512,512]{3,2,0,1:T(8,128)(2,1)} copy(bf16[4,8,512,512]{3,2,1,0:T(8,128)(2,1)} %bitcast.6) | data formatting | bytes 33554432 | tf_op jit(solution)/shard_map/all_to_all | solution.py:24
  640.5 9.3 %fusion.5 = bf16[4,8,16,512]{3,2,0,1:T(8,128)(2,1)S(1)} fusion(bf16[4,8,16,2048]{3,2,0,1:T(8,128)(2,1)} %all-gather.5.cloned.1.call-done, bf16[8,2048,512,1]{2,1,3,0:T(8,128)(2,1)} %bitcast.60), kind=kOutput, calls=%fused_computation.11 | convolution fusion | flops 1074003968 | bytes 19398656 | tf_op jit(solution)/shard_map/secf,efd->secd/dot_general | solution.py:63
  649.8 11.2 %all_to_all.65 = bf16[32,16,512]{2,1,0:T(8,128)(2,1)S(1)} all-to-all(bf16[32,16,512]{2,1,0:T(8,128)(2,1)S(1)} %bitcast.68), channel_id=1, replica_groups=mesh['grp'=2,'fs'=4,'tp'=4] {'tp'}, dimensions={0} | all-to-all | bytes 1048576 | tf_op jit(solution)/shard_map/all_to_all | solution.py:70
  661.0 1.0 convolution_convert_fusion.2
  (13 shorter events, 0.2 us)
Async XLA Ops:
  15.0 37.4 %all-to-all-start.3 = ((bf16[32,16,512]{2,1,0:T(8,128)(2,1)}), bf16[32,16,512]{2,1,0:T(8,128)(2,1)S(1)}, u32[]{:S(2)}, u32[]{:S(2)}) async-start(bf16[32,16,512]{2,1,0:T(8,128)(2,1)} %bitcast.13), calls=%async_computation.3 | async-start | bytes 1048576 | tf_op jit(solution)/shard_map/all_to_all | solution.py:49
  246.6 190.1 %all-to-all-start.1 = ((bf16[32,512,512]{2,1,0:T(8,128)(2,1)}), bf16[32,512,512]{2,1,0:T(8,128)(2,1)}, u32[]{:S(2)}, u32[]{:S(2)}) async-start(bf16[32,512,512]{2,1,0:T(8,128)(2,1)} %get-tuple-element.6), calls=%async_computation.1 | async-start | bytes 33554432 | tf_op jit(solution)/shard_map/all_to_all | solution.py:23
  436.7 190.0 %all-to-all-start.2 = ((bf16[32,512,512]{2,1,0:T(8,128)(2,1)}), bf16[32,512,512]{2,1,0:T(8,128)(2,1)}, u32[]{:S(2)}, u32[]{:S(2)}) async-start(bf16[32,512,512]{2,1,0:T(8,128)(2,1)} %convert_element_type.41), calls=%async_computation.2 | async-start | bytes 33554432 | tf_op jit(solution)/shard_map/all_to_all | solution.py:24
  443.6 51.0 %all-gather.3.cloned.1.call-start = ((), (), s32[]{:S(2)}) async-start(), calls=%async_computation.5 | async-start | bytes 2621440 | tf_op jit(solution)/shard_map/all_gather | solution.py:57
  444.6 195.9 %all-gather.5.cloned.1.call-start = ((), (), s32[]{:S(2)}) async-start(), calls=%async_computation.6 | async-start | bytes 2621440 | tf_op jit(solution)/shard_map/all_gather | solution.py:65
  494.7 9.3 %copy-start = (bf16[4,8,16,2048]{3,2,0,1:T(8,128)(2,1)S(1)}, bf16[4,8,16,2048]{3,2,0,1:T(8,128)(2,1)}, u32[]{:S(2)}) copy-start(bf16[4,8,16,2048]{3,2,0,1:T(8,128)(2,1)} %all-gather.3.cloned.1.call-done) | copy-start | bytes 6291460
Sparse Core Ops, SparseCore 0:
  446.6 48.0 all-gather.2
  512.5 44.4 all-gather.4
where the time goes:
time: 670 us; the launch traced here: 669 us
  waiting for transfers between devices  302 us (45%)
  blocking collectives  205 us (31%)
  other arithmetic  55.9 us (8%)
  local copies, waits for them, and re-layouts  43.6 us (7%)
  matrix products  29.2 us (4%)
  starting transfers between devices  18.4 us (3%)
  between operations  14.2 us (2%)
    all_to_all x1, blocking collectives, local(): lax.all_to_all(gate_local, 'tp', split_axis=0, concat_axis=1, tiled=True)  194 us
    all_to_all x1, waiting for transfers between devices, local(): lax.all_to_all(up_local, 'tp', split_axis=0, concat_axis=1, tiled=True)  166 us
    all_to_all x1, waiting for transfers between devices, local(): lax.all_to_all(down_local, 'tp', split_axis=0, concat_axis=1, tiled=True)  114 us
    convert_element_type x1, other arithmetic, local(): up_local = (up_train * norm_gain[None, :, None]).astype(jnp.bfloat16)  33.2 us
    all_gather x1, waiting for transfers between devices, local(): block_in = lax.all_gather(arrived, 'fs', axis=3, tiled=True)  22.4 us
    convert_element_type x1, other arithmetic, local(): down_local = down_train.astype(jnp.bfloat16)  17.3 us
    all_to_all x1, local copies, waits for them, and re-layouts, local(): lax.all_to_all(gate_local, 'tp', split_axis=0, concat_axis=1, tiled=True)  13.8 us
    all_to_all x1, local copies, waits for them, and re-layouts, local(): lax.all_to_all(up_local, 'tp', split_axis=0, concat_axis=1, tiled=True)  13.8 us
  transfers between devices with their start and end apart: 5, of which 3 were waited for; matrix products, arithmetic and copies ran while one was open for 17% of the time, Pallas kernels for 0%

commit v1 on v0

v1 whole, which is shorter than its diff:
```python
import jax
import jax.numpy as jnp
from jax import lax
from jax.sharding import PartitionSpec as P


CAP = 16
CORES = 2
AHEAD = 3


def parts_of(per):
    return 4 if per % 4 == 0 else 1


def activate(gate_pre, up_pre):
    clamped = jnp.minimum(gate_pre, 7.0)
    bounded = jnp.clip(up_pre, -7.0, 7.0)
    return (clamped * jax.nn.sigmoid(1.702 * clamped) * (bounded + 1.0)).astype(jnp.bfloat16)


def exchange(value, axis, step):
    count = lax.axis_size(axis)
    return lax.ppermute(value, axis, [(i, i ^ step) for i in range(count)])


def gather_fs(block):
    count = lax.axis_size("fs")
    me = lax.axis_index("fs")
    width = block.shape[-1]
    whole = jnp.zeros(block.shape[:-1] + (count * width,), block.dtype)
    zeros = (0,) * (block.ndim - 1)
    for step in range(count):
        piece = block if step == 0 else exchange(block, "fs", step)
        whole = lax.dynamic_update_slice(whole, piece, zeros + ((me ^ step) * width,))
    return whole


def local(tokens, route_expert, route_weight, norm_gain, gate_train, up_train, down_train):
    n = lax.axis_size("tp")
    me = lax.axis_index("tp")
    groups = lax.axis_size("grp")
    grp = lax.axis_index("grp")
    fs_count = lax.axis_size("fs")
    experts, depth, width = gate_train.shape
    per = experts // n
    half = depth // groups
    parts = parts_of(per)
    span = per // parts
    gain = norm_gain[None, :, None]

    def weights(train, scale, first, dest, row, rows):
        piece = lax.dynamic_slice(train, (dest * per + first, row, 0), (span, rows, width))
        if scale is not None:
            piece = piece * lax.dynamic_slice(scale, (0, row, 0), (1, rows, 1))
        return piece.astype(jnp.bfloat16)

    def outgoing(train, scale, part):
        first = part * span
        return [
            weights(train, scale, first, me ^ step, 0, depth)
            if step < CORES
            else weights(train, scale, first, me ^ step, grp * half, half)
            for step in range(n)
        ]

    def blank(count):
        return jnp.zeros((count, n * depth, width), jnp.bfloat16)

    def product(rows, matrix):
        return jnp.einsum("ecd,edf->ecf", rows, matrix, preferred_element_type=jnp.float32)

    trains = (gate_train, up_train, down_train)
    scales = (gain, gain, None)
    first_sent = outgoing(gate_train, gain, 0)
    first_sent[1:], tokens, route_expert = lax.optimization_barrier(
        (first_sent[1:], tokens, route_expert)
    )

    tok_rows, features = tokens.shape
    top = route_expert.shape[1]
    floated = tokens.astype(jnp.float32)
    normed = (
        floated * lax.rsqrt(jnp.mean(floated * floated, axis=-1, keepdims=True) + 1e-06)
    ).astype(jnp.bfloat16)
    flat_expert = route_expert.reshape(-1)
    expert_ids = jnp.arange(experts, dtype=jnp.int32)
    onehot = (flat_expert[:, None] == expert_ids[None, :]).astype(jnp.int32)
    slot_rank = jnp.sum((jnp.cumsum(onehot, axis=0) - 1) * onehot, axis=1)
    slot_index = flat_expert * CAP + slot_rank
    slot_hit = slot_index[:, None] == jnp.arange(experts * CAP, dtype=jnp.int32)[None, :]
    placement = slot_hit.reshape(tok_rows, top, experts * CAP).astype(jnp.float32)
    scatter_mat = jnp.sum(placement, axis=1).astype(jnp.bfloat16)
    combine_mat = jnp.sum(placement * route_weight[:, :, None], axis=1)
    col_width = features // fs_count
    column_part = lax.dynamic_slice_in_dim(
        normed, lax.axis_index("fs") * col_width, col_width, 1
    )
    buffer = lax.dot_general(
        scatter_mat, column_part, (((0,), (0,)), ((), ())), preferred_element_type=jnp.float32
    ).astype(jnp.bfloat16).reshape(n, per, CAP, col_width)
    arrived = []
    for step in range(n):
        block = lax.dynamic_index_in_dim(buffer, me ^ step, 0, keepdims=False)
        arrived.append(block if step == 0 else exchange(block, "tp", step))
    block_in = gather_fs(jnp.concatenate(arrived, axis=1))

    serves = [None, None]
    stages = [(m, part) for m in range(3) for part in range(parts)]
    down_parts, arrivals, filled = [], [], []
    for index, (m, part) in enumerate(stages):
        held = trains[m]
        if index == 0:
            sent = first_sent
        elif index < AHEAD:
            held, sent[1:] = lax.optimization_barrier((held, sent[1:]))
        else:
            held, sent[1:], arrivals[index - AHEAD][-1] = lax.optimization_barrier(
                (held, sent[1:], arrivals[index - AHEAD][-1])
            )
        if index > 0:
            sent = outgoing(held, scales[m], part)
        here = [sent[0]]
        for step in range(1, n):
            here.append(exchange(sent[step], "tp", step))
        arrivals.append(here)
    entry = min(CORES, n - 1)
    pre = []
    for index, (m, part) in enumerate(stages):
        pieces = arrivals[index]
        done = filled[index - 1] if index > 0 else blank(per)
        if part == 0 and m > 0:
            serves[m - 1] = done
            fence = product(block_in, done)
            if index + 1 < len(stages):
                arrivals[index + 1][entry], fence = lax.optimization_barrier(
                    (arrivals[index + 1][entry], fence)
                )
            pre.append(fence)
        base = part * span if m < 2 else 0
        if m < 2:
            out = done if part > 0 or m == 0 else blank(per)
        else:
            out = blank(span)
        for step in range(CORES):
            out = lax.dynamic_update_slice(out, pieces[step], (base, (me ^ step) * depth, 0))
        late = []
        for step in range(CORES, n):
            source = (me ^ step) * depth
            out = lax.dynamic_update_slice(out, pieces[step], (base, source + grp * half, 0))
            for other, row in late:
                out = lax.dynamic_update_slice(out, other, (base, row, 0))
            late = []
            for turn in range(1, groups):
                other = exchange(pieces[step], "grp", turn)
                late.append((other, source + (grp ^ turn) * half))
        for other, row in late:
            out = lax.dynamic_update_slice(out, other, (base, row, 0))
        filled.append(out)
        if m == 2:
            down_parts.append(out)
    gate_serve, up_serve = serves
    down_serve = blank(per)
    hidden = activate(*pre)
    hidden = gather_fs(hidden)
    combine = combine_mat.reshape(tok_rows, n, per, CAP)
    mixed = jnp.zeros((tok_rows, width), jnp.float32)
    for part in range(parts):
        rows = hidden[part * span : (part + 1) * span]
        out = jnp.einsum(
            "ecf,efd->ecd", rows, down_parts[part], preferred_element_type=jnp.float32
        ).astype(jnp.bfloat16)
        back, shares = [], []
        for step in range(n):
            block = out[:, step * CAP : (step + 1) * CAP].reshape(span * CAP, width)
            back.append(block if step == 0 else exchange(block, "tp", step))
            share = lax.dynamic_slice(
                combine, (0, me ^ step, part * span, 0), (tok_rows, 1, span, CAP)
            )
            shares.append(share.reshape(tok_rows, span * CAP))
        mixed = mixed + jnp.dot(
            jnp.concatenate(shares, axis=1),
            jnp.concatenate(back, axis=0).astype(jnp.float32),
            precision=lax.Precision.HIGHEST,
        )
    for part in range(parts):
        down_serve = lax.dynamic_update_slice(down_serve, down_parts[part], (part * span, 0, 0))
    return (gate_serve, up_serve, down_serve, mixed.astype(jnp.bfloat16))


def solution(mesh):
    return jax.shard_map(
        local,
        mesh=mesh,
        in_specs=(
            P(("grp", "tp"), None),
            P(("grp", "tp"), None),
            P(("grp", "tp"), None),
            P("tp"),
            P(None, "tp", "fs"),
            P(None, "tp", "fs"),
            P(None, "tp", "fs"),
        ),
        out_specs=(
            P(("grp", "tp"), None, "fs"),
            P(("grp", "tp"), None, "fs"),
            P(("grp", "tp"), None, "fs"),
            P(("grp", "tp"), "fs"),
        ),
        check_vma=False,
    )
```

time: 670 us -> 505 us (0.75); the launches traced: 669 us -> 495 us
  blocking collectives: 205 us -> 0 us
  waiting for transfers between devices: 302 us -> 241 us
  starting transfers between devices: 18.4 us -> 72.8 us
  local copies, waits for them, and re-layouts: 43.6 us -> 93.7 us
  between operations: 14.2 us -> 1.81 us
    all_to_all x3 -> x0, waiting for transfers between devices: 280 us -> none  [the longest x1 166 us: local(): lax.all_to_all(up_local, 'tp', split_axis=0, concat_axis=1, tiled=True)]
    ppermute x0 -> x81, waiting for transfers between devices: none -> 241 us  [exchange(): return lax.ppermute(value, axis, [(i, i ^ step) for i in range(count)])]
    all_to_all x2 -> x0, blocking collectives: 205 us -> none  [the longest x1 194 us: local(): lax.all_to_all(gate_local, 'tp', split_axis=0, concat_axis=1, tiled=True)]
    ppermute x0 -> x81, starting transfers between devices: none -> 72.8 us  [exchange(): return lax.ppermute(value, axis, [(i, i ^ step) for i in range(count)])]
    dynamic_update_slice x0 -> x73, local copies, waits for them, and re-layouts: none -> 64.7 us  [the longest x15 20.2 us: local(): lax.dynamic_update_slice(out, pieces[step], (base, (me ^ step) * depth, 0))]
    all_to_all x3 -> x0, local copies, waits for them, and re-layouts: 41.5 us -> none  [the longest x1 13.8 us: local(): lax.all_to_all(gate_local, 'tp', split_axis=0, concat_axis=1, tiled=True)]
    all_gather x2 -> x0, waiting for transfers between devices: 22.4 us -> none  [the longest x1 22.4 us: local(): block_in = lax.all_gather(arrived, 'fs', axis=3, tiled=True)]
    all_to_all x3 -> x0, starting transfers between devices: 18.3 us -> none  [the longest x1 7.08 us: local(): lax.all_to_all(up_local, 'tp', split_axis=0, concat_axis=1, tiled=True)]
  transfers between devices with their start and end apart: 5 -> 81, of which waited for: 3 -> 28; matrix products, arithmetic and copies ran while one was open for 17% -> 34% of each run, Pallas kernels for 0% -> 0%
where the time goes in v1:
time: 505 us; the launch traced here: 495 us
  waiting for transfers between devices  241 us (48%)
  local copies, waits for them, and re-layouts  93.7 us (19%)
  starting transfers between devices  72.8 us (14%)
  other arithmetic  59.3 us (12%)
  matrix products  25.9 us (5%)
    ppermute x81, waiting for transfers between devices, exchange(): return lax.ppermute(value, axis, [(i, i ^ step) for i in range(count)])  241 us
    ppermute x81, starting transfers between devices, exchange(): return lax.ppermute(value, axis, [(i, i ^ step) for i in range(count)])  72.8 us
    convert_element_type x16, other arithmetic, weights(): return piece.astype(jnp.bfloat16)  35.5 us
    dynamic_update_slice x15, local copies, waits for them, and re-layouts, local(): lax.dynamic_update_slice(out, pieces[step], (base, (me ^ step) * depth, 0))  20.2 us
    dynamic_update_slice x24, local copies, waits for them, and re-layouts, local(): lax.dynamic_update_slice(out, pieces[step], (base, source + grp * half, 0))  16.3 us
    dot_general x2, matrix products, product(): jnp.einsum('ecd,edf->ecf', rows, matrix, preferred_element_type=jnp.float32)  16.1 us
    dynamic_update_slice x6, other arithmetic, local(): lax.dynamic_update_slice(out, pieces[step], (base, (me ^ step) * depth, 0))  16 us
    convert_element_type x5, local copies, waits for them, and re-layouts, weights(): return piece.astype(jnp.bfloat16)  14.3 us
  transfers between devices with their start and end apart: 81, of which 28 were waited for; matrix products, arithmetic and copies ran while one was open for 34% of the time, Pallas kernels for 0%

profile of v1, /device:TPU:0, one launch (start us, length us, event | category | flops | bytes accessed | tf_op | source)
XLA Modules:
  0.0 494.7 jit_solution(3479999825559253513)
XLA Ops:
  25.9 6.0 %broadcast.54.clone = bf16[8,2048,512]{2,1,0:T(8,128)(2,1)} broadcast(bf16[]{:T(256)} %constant.64.clone.1), dimensions={} | broadcast | bytes 16777218 | tf_op jit(solution)/shard_map/broadcast.6
  53.7 9.8 %collective-permute-done.12 = bf16[2,256,512]{2,1,0:T(8,128)(2,1)S(1)} collective-permute-done((bf16[2,256,512]{2,1,0:T(8,128)(2,1)}, bf16[2,256,512]{2,1,0:T(8,128)(2,1)S(1)}, u32[]{:S(2)}, u32[]{:S(2)}) %collective-permute-start.12) | collective-permute-done | bytes 524320 | tf_op jit(solution)/shard_map/ppermute | solution.py:24
  63.5 3.8 collective-permute-start.32
  73.0 12.7 %collective-permute-done.31 = bf16[8,64,512]{2,1,0:T(8,128)(2,1)S(1)} collective-permute-done((bf16[8,64,512]{2,1,0:T(8,128)(2,1)S(1)}, bf16[8,64,512]{2,1,0:T(8,128)(2,1)S(1)}, u32[]{:S(2)}, u32[]{:S(2)}) %collective-permute-start.31) | collective-permute-done | bytes 524320 | tf_op jit(solution)/shard_map/ppermute | solution.py:24
  91.9 8.6 %collective-permute-done.3 = bf16[2,256,512]{2,1,0:T(8,128)(2,1)S(1)} collective-permute-done((bf16[2,256,512]{2,1,0:T(8,128)(2,1)S(1)}, bf16[2,256,512]{2,1,0:T(8,128)(2,1)S(1)}, u32[]{:S(2)}, u32[]{:S(2)}) %collective-permute-start.3) | collective-permute-done | bytes 524320 | tf_op jit(solution)/shard_map/ppermute | solution.py:24
  101.4 7.3 %collective-permute-done.4 = bf16[2,256,512]{2,1,0:T(8,128)(2,1)S(1)} collective-permute-done((bf16[2,256,512]{2,1,0:T(8,128)(2,1)}, bf16[2,256,512]{2,1,0:T(8,128)(2,1)S(1)}, u32[]{:S(2)}, u32[]{:S(2)}) %collective-permute-start.4) | collective-permute-done | bytes 524320 | tf_op jit(solution)/shard_map/ppermute | solution.py:24
  125.0 5.6 %collective-permute-done.22 = bf16[2,256,512]{2,1,0:T(8,128)(2,1)S(1)} collective-permute-done((bf16[2,256,512]{2,1,0:T(8,128)(2,1)S(1)}, bf16[2,256,512]{2,1,0:T(8,128)(2,1)S(1)}, u32[]{:S(2)}, u32[]{:S(2)}) %collective-permute-start.22) | collective-permute-done | bytes 524320 | tf_op jit(solution)/shard_map/ppermute | solution.py:24
  131.5 10.6 %collective-permute-done.8 = bf16[2,256,512]{2,1,0:T(8,128)(2,1)S(1)} collective-permute-done((bf16[2,256,512]{2,1,0:T(8,128)(2,1)S(1)}, bf16[2,256,512]{2,1,0:T(8,128)(2,1)S(1)}, u32[]{:S(2)}, u32[]{:S(2)}) %collective-permute-start.8) | collective-permute-done | bytes 524320 | tf_op jit(solution)/shard_map/ppermute | solution.py:24
  148.8 3.5 fusion.7
  154.8 10.6 %collective-permute-done.33 = bf16[2,256,512]{2,1,0:T(8,128)(2,1)} collective-permute-done((bf16[2,256,512]{2,1,0:T(8,128)(2,1)S(1)}, bf16[2,256,512]{2,1,0:T(8,128)(2,1)}, u32[]{:S(2)}, u32[]{:S(2)}) %collective-permute-start.33) | collective-permute-done | bytes 524320 | tf_op jit(solution)/shard_map/ppermute | solution.py:24
  174.2 3.6 fusion.11
  178.9 12.8 %collective-permute-done.13 = bf16[2,256,512]{2,1,0:T(8,128)(2,1)S(1)} collective-permute-done((bf16[2,256,512]{2,1,0:T(8,128)(2,1)S(1)}, bf16[2,256,512]{2,1,0:T(8,128)(2,1)S(1)}, u32[]{:S(2)}, u32[]{:S(2)}) %collective-permute-start.13) | collective-permute-done | bytes 524320 | tf_op jit(solution)/shard_map/ppermute | solution.py:24
  195.6 10.9 %collective-permute-done.23 = bf16[2,256,512]{2,1,0:T(8,128)(2,1)S(1)} collective-permute-done((bf16[2,256,512]{2,1,0:T(8,128)(2,1)S(1)}, bf16[2,256,512]{2,1,0:T(8,128)(2,1)S(1)}, u32[]{:S(2)}, u32[]{:S(2)}) %collective-permute-start.23) | collective-permute-done | bytes 524320 | tf_op jit(solution)/shard_map/ppermute | solution.py:24
  209.7 8.1 %collective-permute-done.24 = bf16[2,256,512]{2,1,0:T(8,128)(2,1)S(1)} collective-permute-done((bf16[2,256,512]{2,1,0:T(8,128)(2,1)S(1)}, bf16[2,256,512]{2,1,0:T(8,128)(2,1)S(1)}, u32[]{:S(2)}, u32[]{:S(2)}) %collective-permute-start.24) | collective-permute-done | bytes 524320 | tf_op jit(solution)/shard_map/ppermute | solution.py:24
  219.3 3.5 fusion.8
  225.5 12.9 %collective-permute-done.18 = bf16[2,256,512]{2,1,0:T(8,128)(2,1)S(1)} collective-permute-done((bf16[2,256,512]{2,1,0:T(8,128)(2,1)S(1)}, bf16[2,256,512]{2,1,0:T(8,128)(2,1)S(1)}, u32[]{:S(2)}, u32[]{:S(2)}) %collective-permute-start.18) | collective-permute-done | bytes 524320 | tf_op jit(solution)/shard_map/ppermute | solution.py:24
  241.8 8.8 %fusion.93 = f32[8,64,512]{2,1,0:T(8,128)S(1)} fusion(bf16[8,64,2048]{2,1,0:T(8,128)(2,1)S(1)} %constant_dynamic-update-slice_fusion.41, bf16[8,2048,512]{2,1,0:T(8,128)(2,1)} %constant_dynamic-update-slice_fusion.51), kind=kOutput, calls=%fused_computation.254 | convolution fusion | flops 1073741824 | bytes 19922944 | tf_op jit(solution)/shard_map/ecd,edf->ecf/dot_general | solution.py:71
  257.9 3.5 fusion.12
  267.5 3.5 fusion.13
  271.0 3.7 collective-permute-done.48
  282.0 3.6 dynamic-slice_convert_fusion
  285.6 15.2 %collective-permute-done.34 = bf16[2,256,512]{2,1,0:T(8,128)(2,1)S(1)} collective-permute-done((bf16[2,256,512]{2,1,0:T(8,128)(2,1)}, bf16[2,256,512]{2,1,0:T(8,128)(2,1)S(1)}, u32[]{:S(2)}, u32[]{:S(2)}) %collective-permute-start.34) | collective-permute-done | bytes 524320 | tf_op jit(solution)/shard_map/ppermute | solution.py:24
  306.3 19.9 %collective-permute-done.39 = bf16[2,256,512]{2,1,0:T(8,128)(2,1)S(1)} collective-permute-done((bf16[2,256,512]{2,1,0:T(8,128)(2,1)S(1)}, bf16[2,256,512]{2,1,0:T(8,128)(2,1)S(1)}, u32[]{:S(2)}, u32[]{:S(2)}) %collective-permute-start.39) | collective-permute-done | bytes 524320 | tf_op jit(solution)/shard_map/ppermute | solution.py:24
  332.2 19.5 %collective-permute-done.44 = bf16[2,256,512]{2,1,0:T(8,128)(2,1)S(1)} collective-permute-done((bf16[2,256,512]{2,1,0:T(8,128)(2,1)S(1)}, bf16[2,256,512]{2,1,0:T(8,128)(2,1)S(1)}, u32[]{:S(2)}, u32[]{:S(2)}) %collective-permute-start.44) | collective-permute-done | bytes 524320 | tf_op jit(solution)/shard_map/ppermute | solution.py:24
  354.5 7.3 %fusion.94 = f32[8,64,512]{2,1,0:T(8,128)} fusion(bf16[8,64,2048]{2,1,0:T(8,128)(2,1)} %copy-done.3, bf16[8,2048,512]{2,1,0:T(8,128)(2,1)S(1)} %constant_dynamic-update-slice_fusion.27), kind=kOutput, calls=%fused_computation.255 | convolution fusion | flops 1073741824 | bytes 19922944 | tf_op jit(solution)/shard_map/ecd,edf->ecf/dot_general | solution.py:71
  370.7 4.8 collective-permute-done.49
  380.5 7.4 %dynamic_update_slice.310 = bf16[8,2048,512]{2,1,0:T(8,128)(2,1)} pad(bf16[2,2048,512]{2,1,0:T(8,128)(2,1)} %constant_dynamic-update-slice_fusion.22, bf16[]{:T(256)} %constant.64.clone.1), padding=0_6x0_0x0_0 | pad | bytes 20971522 | tf_op jit(solution)/shard_map/dynamic_update_slice | solution.py:187
  392.8 5.9 %collective-permute-done.58 = bf16[2,256,512]{2,1,0:T(8,128)(2,1)S(1)} collective-permute-done((bf16[2,256,512]{2,1,0:T(8,128)(2,1)}, bf16[2,256,512]{2,1,0:T(8,128)(2,1)S(1)}, u32[]{:S(2)}, u32[]{:S(2)}) %collective-permute-start.58) | collective-permute-done | bytes 524320 | tf_op jit(solution)/shard_map/ppermute | solution.py:24
  406.5 10.4 %collective-permute-done.55 = bf16[2,256,512]{2,1,0:T(8,128)(2,1)S(1)} collective-permute-done((bf16[2,256,512]{2,1,0:T(8,128)(2,1)S(1)}, bf16[2,256,512]{2,1,0:T(8,128)(2,1)S(1)}, u32[]{:S(2)}, u32[]{:S(2)}) %collective-permute-start.55) | collective-permute-done | bytes 524320 | tf_op jit(solution)/shard_map/ppermute | solution.py:24
  417.0 11.2 %collective-permute-done.59 = bf16[2,256,512]{2,1,0:T(8,128)(2,1)S(1)} collective-permute-done((bf16[2,256,512]{2,1,0:T(8,128)(2,1)S(1)}, bf16[2,256,512]{2,1,0:T(8,128)(2,1)S(1)}, u32[]{:S(2)}, u32[]{:S(2)}) %collective-permute-start.59) | collective-permute-done | bytes 524320 | tf_op jit(solution)/shard_map/ppermute | solution.py:24
  428.6 10.8 %collective-permute-done.60 = bf16[2,256,512]{2,1,0:T(8,128)(2,1)S(1)} collective-permute-done((bf16[2,256,512]{2,1,0:T(8,128)(2,1)S(1)}, bf16[2,256,512]{2,1,0:T(8,128)(2,1)S(1)}, u32[]{:S(2)}, u32[]{:S(2)}) %collective-permute-start.60) | collective-permute-done | bytes 524320 | tf_op jit(solution)/shard_map/ppermute | solution.py:24
  445.1 20.2 %collective-permute-done.67 = bf16[8,64,512]{2,1,0:T(8,128)(2,1)S(1)} collective-permute-done((bf16[8,64,512]{2,1,0:T(8,128)(2,1)S(1)}, bf16[8,64,512]{2,1,0:T(8,128)(2,1)S(1)}, u32[]{:S(2)}, u32[]{:S(2)}) %collective-permute-start.67) | collective-permute-done | bytes 524320 | tf_op jit(solution)/shard_map/ppermute | solution.py:24
  (330 shorter events, 206.9 us)
Async XLA Ops:
  6.0 36.4 %collective-permute-start.2 = (bf16[2,256,512]{2,1,0:T(8,128)(2,1)}, bf16[2,256,512]{2,1,0:T(8,128)(2,1)}, u32[]{:S(2)}, u32[]{:S(2)}) collective-permute-start(bf16[2,256,512]{2,1,0:T(8,128)(2,1)} %get-tuple-element.35), channel_id=1, source_target_pairs={{0,3},{1,2},{2,1},{3,0},{4,7},{5,6},{6,5},{7,4},{8,11},{9,10},{10,... | collective-permute-start | bytes 1572872 | tf_op jit(solution)/shard_map/ppermute | solution.py:24
  11.1 36.4 %collective-permute-start.7 = (bf16[2,256,512]{2,1,0:T(8,128)(2,1)}, bf16[2,256,512]{2,1,0:T(8,128)(2,1)}, u32[]{:S(2)}, u32[]{:S(2)}) collective-permute-start(bf16[2,256,512]{2,1,0:T(8,128)(2,1)} %get-tuple-element.78), channel_id=1, source_target_pairs={{0,3},{1,2},{2,1},{3,0},{4,7},{5,6},{6,5},{7,4},{8,11},{9,10},{10,... | collective-permute-start | bytes 1572872 | tf_op jit(solution)/shard_map/ppermute | solution.py:24
  38.3 49.7 %collective-permute-start = (bf16[2,512,512]{2,1,0:T(8,128)(2,1)S(1)}, bf16[2,512,512]{2,1,0:T(8,128)(2,1)S(1)}, u32[]{:S(2)}, u32[]{:S(2)}) collective-permute-start(bf16[2,512,512]{2,1,0:T(8,128)(2,1)S(1)} %multiply_convert_fusion.14), channel_id=1, source_target_pairs={{0,1},{1,0},{2,3},{3,2},{4,5},{5,4},{6,7},{7,6},{8,9},{9,8},{10,11... | collective-permute-start | bytes 3145736 | tf_op jit(solution)/shard_map/ppermute | solution.py:24
  38.7 32.7 %collective-permute-start.1 = (bf16[2,256,512]{2,1,0:T(8,128)(2,1)}, bf16[2,256,512]{2,1,0:T(8,128)(2,1)S(1)}, u32[]{:S(2)}, u32[]{:S(2)}) collective-permute-start(bf16[2,256,512]{2,1,0:T(8,128)(2,1)} %get-tuple-element.34), channel_id=1, source_target_pairs={{0,2},{1,3},{2,0},{3,1},{4,6},{5,7},{6,4},{7,5},{8,10},{9,11},{10,... | collective-permute-start | bytes 1572872 | tf_op jit(solution)/shard_map/ppermute | solution.py:24
  42.3 28.5 %collective-permute-start.30 = (bf16[8,64,512]{2,1,0:T(8,128)(2,1)S(1)}, bf16[8,64,512]{2,1,0:T(8,128)(2,1)S(1)}, u32[]{:S(2)}, u32[]{:S(2)}) collective-permute-start(bf16[8,64,512]{2,1,0:T(8,128)(2,1)S(1)} %get-tuple-element.98), channel_id=1, source_target_pairs={{0,4},{4,0},{8,12},{12,8},{1,5},{5,1},{9,13},{13,9},{2,6},{6,2},{1... | collective-permute-start | bytes 1572872 | tf_op jit(solution)/shard_map/ppermute | solution.py:24
  47.5 38.2 %collective-permute-start.31 = (bf16[8,64,512]{2,1,0:T(8,128)(2,1)S(1)}, bf16[8,64,512]{2,1,0:T(8,128)(2,1)S(1)}, u32[]{:S(2)}, u32[]{:S(2)}) collective-permute-start(bf16[8,64,512]{2,1,0:T(8,128)(2,1)S(1)} %get-tuple-element.98), channel_id=1, source_target_pairs={{0,8},{4,12},{8,0},{12,4},{1,9},{5,13},{9,1},{13,5},{2,10},{6,14},... | collective-permute-start | bytes 1572872 | tf_op jit(solution)/shard_map/ppermute | solution.py:24
  70.8 47.2 %collective-permute-start.5 = (bf16[2,512,512]{2,1,0:T(8,128)(2,1)}, bf16[2,512,512]{2,1,0:T(8,128)(2,1)S(1)}, u32[]{:S(2)}, u32[]{:S(2)}) collective-permute-start(bf16[2,512,512]{2,1,0:T(8,128)(2,1)} %multiply_convert_fusion.13), channel_id=1, source_target_pairs={{0,1},{1,0},{2,3},{3,2},{4,5},{5,4},{6,7},{7,6},{8,9},{9,8},{10,11... | collective-permute-start | bytes 3145736 | tf_op jit(solution)/shard_map/ppermute | solution.py:24
  71.4 45.1 %collective-permute-start.6 = (bf16[2,256,512]{2,1,0:T(8,128)(2,1)}, bf16[2,256,512]{2,1,0:T(8,128)(2,1)S(1)}, u32[]{:S(2)}, u32[]{:S(2)}) collective-permute-start(bf16[2,256,512]{2,1,0:T(8,128)(2,1)} %get-tuple-element.79), channel_id=1, source_target_pairs={{0,2},{1,3},{2,0},{3,1},{4,6},{5,7},{6,4},{7,5},{8,10},{9,11},{10,... | collective-permute-start | bytes 1572872 | tf_op jit(solution)/shard_map/ppermute | solution.py:24
  100.5 67.6 %collective-permute-start.10 = (bf16[2,512,512]{2,1,0:T(8,128)(2,1)S(1)}, bf16[2,512,512]{2,1,0:T(8,128)(2,1)S(1)}, u32[]{:S(2)}, u32[]{:S(2)}) collective-permute-start(bf16[2,512,512]{2,1,0:T(8,128)(2,1)S(1)} %multiply_convert_fusion.12), channel_id=1, source_target_pairs={{0,1},{1,0},{2,3},{3,2},{4,5},{5,4},{6,7},{7,6},{8,9},{9,8},{10,11... | collective-permute-start | bytes 3145736 | tf_op jit(solution)/shard_map/ppermute | solution.py:24
  108.6 58.0 %collective-permute-start.11 = (bf16[2,256,512]{2,1,0:T(8,128)(2,1)S(1)}, bf16[2,256,512]{2,1,0:T(8,128)(2,1)S(1)}, u32[]{:S(2)}, u32[]{:S(2)}) collective-permute-start(bf16[2,256,512]{2,1,0:T(8,128)(2,1)S(1)} %copy-done.9), channel_id=1, source_target_pairs={{0,2},{1,3},{2,0},{3,1},{4,6},{5,7},{6,4},{7,5},{8,10},{9,11},{10,... | collective-permute-start | bytes 1572872 | tf_op jit(solution)/shard_map/ppermute | solution.py:24
  130.7 64.7 %collective-permute-start.20 = (bf16[2,512,512]{2,1,0:T(8,128)(2,1)S(1)}, bf16[2,512,512]{2,1,0:T(8,128)(2,1)S(1)}, u32[]{:S(2)}, u32[]{:S(2)}) collective-permute-start(bf16[2,512,512]{2,1,0:T(8,128)(2,1)S(1)} %multiply_convert_fusion.8), channel_id=1, source_target_pairs={{0,1},{1,0},{2,3},{3,2},{4,5},{5,4},{6,7},{7,6},{8,9},{9,8},{10,11... | collective-permute-start | bytes 3145736 | tf_op jit(solution)/shard_map/ppermute | solution.py:24
  142.2 35.6 %collective-permute-start.21 = (bf16[2,256,512]{2,1,0:T(8,128)(2,1)S(1)}, bf16[2,256,512]{2,1,0:T(8,128)(2,1)S(1)}, u32[]{:S(2)}, u32[]{:S(2)}) collective-permute-start(bf16[2,256,512]{2,1,0:T(8,128)(2,1)S(1)} %get-tuple-element.73), channel_id=1, source_target_pairs={{0,2},{1,3},{2,0},{3,1},{4,6},{5,7},{6,4},{7,5},{8,10},{9,11},{10,... | collective-permute-start | bytes 1572872 | tf_op jit(solution)/shard_map/ppermute | solution.py:24
  165.4 57.4 %collective-permute-start.15 = (bf16[2,512,512]{2,1,0:T(8,128)(2,1)S(1)}, bf16[2,512,512]{2,1,0:T(8,128)(2,1)S(1)}, u32[]{:S(2)}, u32[]{:S(2)}) collective-permute-start(bf16[2,512,512]{2,1,0:T(8,128)(2,1)S(1)} %multiply_convert_fusion.10), channel_id=1, source_target_pairs={{0,1},{1,0},{2,3},{3,2},{4,5},{5,4},{6,7},{7,6},{8,9},{9,8},{10,11... | collective-permute-start | bytes 3145736 | tf_op jit(solution)/shard_map/ppermute | solution.py:24
  177.7 30.4 %collective-permute-start.16 = (bf16[2,256,512]{2,1,0:T(8,128)(2,1)S(1)}, bf16[2,256,512]{2,1,0:T(8,128)(2,1)S(1)}, u32[]{:S(2)}, u32[]{:S(2)}) collective-permute-start(bf16[2,256,512]{2,1,0:T(8,128)(2,1)S(1)} %get-tuple-element.75), channel_id=1, source_target_pairs={{0,2},{1,3},{2,0},{3,1},{4,6},{5,7},{6,4},{7,5},{8,10},{9,11},{10,... | collective-permute-start | bytes 1572872 | tf_op jit(solution)/shard_map/ppermute | solution.py:24
  195.4 80.7 %collective-permute-start.25 = (bf16[2,512,512]{2,1,0:T(8,128)(2,1)S(1)}, bf16[2,512,512]{2,1,0:T(8,128)(2,1)S(1)}, u32[]{:S(2)}, u32[]{:S(2)}) collective-permute-start(bf16[2,512,512]{2,1,0:T(8,128)(2,1)S(1)} %multiply_convert_fusion.6), channel_id=1, source_target_pairs={{0,1},{1,0},{2,3},{3,2},{4,5},{5,4},{6,7},{7,6},{8,9},{9,8},{10,11... | collective-permute-start | bytes 3145736 | tf_op jit(solution)/shard_map/ppermute | solution.py:24
  206.5 48.5 %collective-permute-start.26 = (bf16[2,256,512]{2,1,0:T(8,128)(2,1)S(1)}, bf16[2,256,512]{2,1,0:T(8,128)(2,1)}, u32[]{:S(2)}, u32[]{:S(2)}) collective-permute-start(bf16[2,256,512]{2,1,0:T(8,128)(2,1)S(1)} %get-tuple-element.71), channel_id=1, source_target_pairs={{0,2},{1,3},{2,0},{3,1},{4,6},{5,7},{6,4},{7,5},{8,10},{9,11},{10,... | collective-permute-start | bytes 1572872 | tf_op jit(solution)/shard_map/ppermute | solution.py:24
  208.1 31.3 %collective-permute-start.19 = (bf16[2,256,512]{2,1,0:T(8,128)(2,1)S(1)}, bf16[2,256,512]{2,1,0:T(8,128)(2,1)S(1)}, u32[]{:S(2)}, u32[]{:S(2)}) collective-permute-start(bf16[2,256,512]{2,1,0:T(8,128)(2,1)S(1)} %collective-permute-done.17), channel_id=1, source_target_pairs={{0,16},{16,0},{1,17},{17,1},{2,18},{18,2},{3,19},{19,3},{4,20},{20... | collective-permute-start | bytes 1572872 | tf_op jit(solution)/shard_map/ppermute | solution.py:24
  222.8 82.0 %collective-permute-start.36 = (bf16[2,512,512]{2,1,0:T(8,128)(2,1)}, bf16[2,512,512]{2,1,0:T(8,128)(2,1)}, u32[]{:S(2)}, u32[]{:S(2)}) collective-permute-start(bf16[2,512,512]{2,1,0:T(8,128)(2,1)} %multiply_convert_fusion.4), channel_id=1, source_target_pairs={{0,1},{1,0},{2,3},{3,2},{4,5},{5,4},{6,7},{7,6},{8,9},{9,8},{10,11... | collective-permute-start | bytes 3145736 | tf_op jit(solution)/shard_map/ppermute | solution.py:24
  255.0 47.4 %collective-permute-start.37 = (bf16[2,256,512]{2,1,0:T(8,128)(2,1)}, bf16[2,256,512]{2,1,0:T(8,128)(2,1)S(1)}, u32[]{:S(2)}, u32[]{:S(2)}) collective-permute-start(bf16[2,256,512]{2,1,0:T(8,128)(2,1)} %get-tuple-element.69), channel_id=1, source_target_pairs={{0,2},{1,3},{2,0},{3,1},{4,6},{5,7},{6,4},{7,5},{8,10},{9,11},{10,... | collective-permute-start | bytes 1572872 | tf_op jit(solution)/shard_map/ppermute | solution.py:24
  263.4 68.6 %collective-permute-start.41 = (bf16[2,512,512]{2,1,0:T(8,128)(2,1)}, bf16[2,512,512]{2,1,0:T(8,128)(2,1)S(1)}, u32[]{:S(2)}, u32[]{:S(2)}) collective-permute-start(bf16[2,512,512]{2,1,0:T(8,128)(2,1)} %multiply_convert_fusion.2), channel_id=1, source_target_pairs={{0,1},{1,0},{2,3},{3,2},{4,5},{5,4},{6,7},{7,6},{8,9},{9,8},{10,11... | collective-permute-start | bytes 3145736 | tf_op jit(solution)/shard_map/ppermute | solution.py:24
  300.9 28.7 %collective-permute-start.40 = (bf16[2,256,512]{2,1,0:T(8,128)(2,1)}, bf16[2,256,512]{2,1,0:T(8,128)(2,1)S(1)}, u32[]{:S(2)}, u32[]{:S(2)}) collective-permute-start(bf16[2,256,512]{2,1,0:T(8,128)(2,1)} %copy-done.7), channel_id=1, source_target_pairs={{0,16},{16,0},{1,17},{17,1},{2,18},{18,2},{3,19},{19,3},{4,20},{20... | collective-permute-start | bytes 1572872 | tf_op jit(solution)/shard_map/ppermute | solution.py:24
  304.8 58.7 %collective-permute-start.46 = (bf16[2,512,512]{2,1,0:T(8,128)(2,1)}, bf16[2,512,512]{2,1,0:T(8,128)(2,1)}, u32[]{:S(2)}, u32[]{:S(2)}) collective-permute-start(bf16[2,512,512]{2,1,0:T(8,128)(2,1)} %get-tuple-element.93), channel_id=1, source_target_pairs={{0,1},{1,0},{2,3},{3,2},{4,5},{5,4},{6,7},{7,6},{8,9},{9,8},{10,11... | collective-permute-start | bytes 3145736 | tf_op jit(solution)/shard_map/ppermute | solution.py:24
  331.9 68.3 %collective-permute-start.51 = (bf16[2,512,512]{2,1,0:T(8,128)(2,1)}, bf16[2,512,512]{2,1,0:T(8,128)(2,1)}, u32[]{:S(2)}, u32[]{:S(2)}) collective-permute-start(bf16[2,512,512]{2,1,0:T(8,128)(2,1)} %get-tuple-element.89), channel_id=1, source_target_pairs={{0,1},{1,0},{2,3},{3,2},{4,5},{5,4},{6,7},{7,6},{8,9},{9,8},{10,11... | collective-permute-start | bytes 3145736 | tf_op jit(solution)/shard_map/ppermute | solution.py:24
  363.6 39.6 %collective-permute-start.56 = (bf16[2,512,512]{2,1,0:T(8,128)(2,1)}, bf16[2,512,512]{2,1,0:T(8,128)(2,1)S(1)}, u32[]{:S(2)}, u32[]{:S(2)}) collective-permute-start(bf16[2,512,512]{2,1,0:T(8,128)(2,1)} %get-tuple-element.87), channel_id=1, source_target_pairs={{0,1},{1,0},{2,3},{3,2},{4,5},{5,4},{6,7},{7,6},{8,9},{9,8},{10,11... | collective-permute-start | bytes 3145736 | tf_op jit(solution)/shard_map/ppermute | solution.py:24
  398.7 29.5 %collective-permute-start.59 = (bf16[2,256,512]{2,1,0:T(8,128)(2,1)S(1)}, bf16[2,256,512]{2,1,0:T(8,128)(2,1)S(1)}, u32[]{:S(2)}, u32[]{:S(2)}) collective-permute-start(bf16[2,256,512]{2,1,0:T(8,128)(2,1)S(1)} %collective-permute-done.57), channel_id=1, source_target_pairs={{0,16},{16,0},{1,17},{17,1},{2,18},{18,2},{3,19},{19,3},{4,20},{20... | collective-permute-start | bytes 1572872 | tf_op jit(solution)/shard_map/ppermute | solution.py:24
  400.2 39.2 %collective-permute-start.60 = (bf16[2,256,512]{2,1,0:T(8,128)(2,1)S(1)}, bf16[2,256,512]{2,1,0:T(8,128)(2,1)S(1)}, u32[]{:S(2)}, u32[]{:S(2)}) collective-permute-start(bf16[2,256,512]{2,1,0:T(8,128)(2,1)S(1)} %collective-permute-done.58), channel_id=1, source_target_pairs={{0,16},{16,0},{1,17},{17,1},{2,18},{18,2},{3,19},{19,3},{4,20},{20... | collective-permute-start | bytes 1572872 | tf_op jit(solution)/shard_map/ppermute | solution.py:24
  403.2 38.9 %collective-permute-start.62 = (bf16[2,256,512]{2,1,0:T(8,128)(2,1)S(1)}, bf16[2,256,512]{2,1,0:T(8,128)(2,1)S(1)}, u32[]{:S(2)}, u32[]{:S(2)}) collective-permute-start(bf16[2,256,512]{2,1,0:T(8,128)(2,1)S(1)} %copy-done.13), channel_id=1, source_target_pairs={{0,2},{1,3},{2,0},{3,1},{4,6},{5,7},{6,4},{7,5},{8,10},{9,11},{10,... | collective-permute-start | bytes 1572872 | tf_op jit(solution)/shard_map/ppermute | solution.py:24
  405.7 36.4 %collective-permute-start.63 = (bf16[2,256,512]{2,1,0:T(8,128)(2,1)S(1)}, bf16[2,256,512]{2,1,0:T(8,128)(2,1)S(1)}, u32[]{:S(2)}, u32[]{:S(2)}) collective-permute-start(bf16[2,256,512]{2,1,0:T(8,128)(2,1)S(1)} %copy-done.12), channel_id=1, source_target_pairs={{0,3},{1,2},{2,1},{3,0},{4,7},{5,6},{6,5},{7,4},{8,11},{9,10},{10,... | collective-permute-start | bytes 1572872 | tf_op jit(solution)/shard_map/ppermute | solution.py:24
  428.2 37.2 %collective-permute-start.67 = (bf16[8,64,512]{2,1,0:T(8,128)(2,1)S(1)}, bf16[8,64,512]{2,1,0:T(8,128)(2,1)S(1)}, u32[]{:S(2)}, u32[]{:S(2)}) collective-permute-start(bf16[8,64,512]{2,1,0:T(8,128)(2,1)S(1)} %get-tuple-element.65), channel_id=1, source_target_pairs={{0,8},{4,12},{8,0},{12,4},{1,9},{5,13},{9,1},{13,5},{2,10},{6,14},... | collective-permute-start | bytes 1572872 | tf_op jit(solution)/shard_map/ppermute | solution.py:24
  442.0 31.7 %collective-permute-start.61 = (bf16[2,512,512]{2,1,0:T(8,128)(2,1)}, bf16[2,512,512]{2,1,0:T(8,128)(2,1)S(1)}, u32[]{:S(2)}, u32[]{:S(2)}) collective-permute-start(bf16[2,512,512]{2,1,0:T(8,128)(2,1)} %get-tuple-element.84), channel_id=1, source_target_pairs={{0,1},{1,0},{2,3},{3,2},{4,5},{5,4},{6,7},{7,6},{8,9},{9,8},{10,11... | collective-permute-start | bytes 3145736 | tf_op jit(solution)/shard_map/ppermute | solution.py:24
  442.1 33.7 %collective-permute-start.64 = (bf16[2,256,512]{2,1,0:T(8,128)(2,1)S(1)}, bf16[2,256,512]{2,1,0:T(8,128)(2,1)S(1)}, u32[]{:S(2)}, u32[]{:S(2)}) collective-permute-start(bf16[2,256,512]{2,1,0:T(8,128)(2,1)S(1)} %collective-permute-done.62), channel_id=1, source_target_pairs={{0,16},{16,0},{1,17},{17,1},{2,18},{18,2},{3,19},{19,3},{4,20},{20... | collective-permute-start | bytes 1572872 | tf_op jit(solution)/shard_map/ppermute | solution.py:24
  443.7 34.0 %collective-permute-start.65 = (bf16[2,256,512]{2,1,0:T(8,128)(2,1)S(1)}, bf16[2,256,512]{2,1,0:T(8,128)(2,1)S(1)}, u32[]{:S(2)}, u32[]{:S(2)}) collective-permute-start(bf16[2,256,512]{2,1,0:T(8,128)(2,1)S(1)} %collective-permute-done.63), channel_id=1, source_target_pairs={{0,16},{16,0},{1,17},{17,1},{2,18},{18,2},{3,19},{19,3},{4,20},{20... | collective-permute-start | bytes 1572872 | tf_op jit(solution)/shard_map/ppermute | solution.py:24
  (76 other events, 1653.1 us)
